TPU v7x, 256 devices: a whole 4x4x8 slice. The times are simulated.
256 devices in a mesh: fs: 32 (over z, x), tp: 8 (over y, core).
Axes of the slice: x: 4, y: 4, z: 8, core: 2. Of those that a mesh axis runs over, the one named last changes fastest.
Arguments:
- tokens: bfloat16 [32768, 2048], P('fs', 'tp'), may hold values from -6 to 6
- grad_out: bfloat16 [32768, 2048], P('fs', 'tp'), may hold values from -6 to 6
- norm_gain: float32 [2048], replicated, may hold values from 0.1 to 1.9
- gate_weight: bfloat16 [3072, 2048], P('tp', 'fs'), may hold values from -0.125 to 0.125
- up_weight: bfloat16 [3072, 2048], P('tp', 'fs'), may hold values from -0.125 to 0.125
- down_weight: bfloat16 [3072, 2048], P('tp', 'fs'), may hold values from -0.109375 to 0.109375
Outputs:
- grad_input: bfloat16 [32768, 2048], P('fs', 'tp')
- grad_gate: float32 [3072, 2048], P('tp', 'fs')
- grad_up: float32 [3072, 2048], P('tp', 'fs')
- grad_down: float32 [3072, 2048], P('tp', 'fs')
- row_squares: float32 [3, 3072], P(None, 'tp')
All inputs are finite; a program needn't handle non-finite values.
Results may differ from a plain program's by a relative error of at most 0.015.
Values may be sent and summed in bfloat16 or wider, within the bound.
A program may use at most 64 MiB of HBM per device.

v0:
```python
import jax
import jax.numpy as jnp
from jax import lax
from jax.sharding import Mesh
from jax.sharding import PartitionSpec as P

FS = ("fs_0", "fs_1")


def sent_together(arrays, axis, dim, along):
    widths = [a.shape[along] for a in arrays]
    both = jnp.concatenate(arrays, axis=along)
    whole = lax.all_gather(both, axis, axis=dim, tiled=True)
    return tuple(jnp.split(whole, [sum(widths[:k]) for k in range(1, len(widths))], axis=along))


def gather_turned(arrays, axis, dims):
    turned = [jnp.moveaxis(a, dim, 0) for a, dim in zip(arrays, dims)]
    widths = [t[0].size for t in turned]
    both = jnp.concatenate([t.reshape(-1, w) for t, w in zip(turned, widths)], axis=1)
    whole = lax.all_gather(both, axis, axis=0, tiled=True)
    parts = jnp.split(whole, [sum(widths[:k]) for k in range(1, len(widths))], axis=1)
    return tuple(
        (
            jnp.moveaxis(b.reshape(-1, *t.shape[1:]), 0, dim)
            for b, t, dim in zip(parts, turned, dims)
        )
    )


def summed_rows(x, axes, dim):
    if not axes:
        return x
    nearer = lax.psum_scatter(x, axes[0], scatter_dimension=dim, tiled=True)
    return summed_rows(nearer, axes[1:], dim)


def in_blocks(x, dim, peers):
    before, after = (x.shape[:dim], x.shape[dim + 1 :])
    return jnp.moveaxis(x.reshape(*before, peers, -1, *after), dim, 0)


def sum_at_owner(x, axis, dim):
    peers = lax.axis_size(axis)
    parts = lax.all_to_all(in_blocks(x, dim, peers), axis, 0, 0, tiled=True)
    return jnp.sum(parts.astype(jnp.float32), axis=0)


def copy_for_each(x, axis):
    peers = lax.axis_size(axis)
    return lax.all_to_all(jnp.broadcast_to(x[None], (peers, *x.shape)), axis, 0, 0, tiled=True)


def taken_together(x, axis):
    everything = copy_for_each(x, axis)
    return jnp.sum(everything, axis=0)


def in_one(arrays, axis):
    line, at, gathered = (jnp.concatenate([a.reshape(-1) for a in arrays]), 0, [])
    total = taken_together(line, axis)
    for a in arrays:
        gathered.append(total[at : at + a.size].reshape(a.shape))
        at += a.size
    return tuple(gathered)


def contract(left, right, left_dim, right_dim):
    return lax.dot_general(
        left, right, (((left_dim,), (right_dim,)), ((), ())), preferred_element_type=jnp.float32
    )


def rms_back(grad_rows, unit_rows, inv_rms, gain_rows):
    scaled = gain_rows * grad_rows
    inner = jnp.mean(scaled * unit_rows, axis=-1, keepdims=True)
    return inv_rms * (scaled - unit_rows * inner)


def on_device(tokens, grad_out, norm_gain, gate_weight, up_weight, down_weight):
    full_tokens, full_grad = sent_together((tokens, grad_out), "tp", 1, 0)
    floated = full_tokens.astype(jnp.float32)
    inv_rms = lax.rsqrt(jnp.mean(floated * floated, axis=-1, keepdims=True) + 1e-06)
    unit_rows = floated * inv_rms
    gain_rows = norm_gain[None, :]
    normed = (unit_rows * gain_rows).astype(jnp.bfloat16)
    gate_full, up_full, down_full = gather_turned(
        (gate_weight, up_weight, down_weight), FS, (1, 1, 1)
    )
    grad_hidden = 0.5 * contract(full_grad, down_full, 1, 1)
    factor = (full_tokens.shape[0] * lax.axis_size(FS)) ** (-0.5)
    gate_pre = contract(normed, gate_full, 1, 1)
    up_pre = contract(normed, up_full, 1, 1)
    sigma = jax.nn.sigmoid(gate_pre)
    active = gate_pre * sigma
    hidden = (active * up_pre).astype(jnp.bfloat16)
    term_down = 0.5 * factor * contract(hidden, full_grad, 0, 0)
    grad_down = summed_rows(term_down.astype(jnp.bfloat16), FS, 1).astype(jnp.float32)
    gate_grad_pre = (grad_hidden * up_pre * sigma * (1.0 + gate_pre * (1.0 - sigma))).astype(
        jnp.bfloat16
    )
    term_gate = factor * contract(gate_grad_pre, normed, 0, 0)
    grad_gate = summed_rows(term_gate.astype(jnp.bfloat16), FS, 1).astype(jnp.float32)
    up_grad_pre = (grad_hidden * active).astype(jnp.bfloat16)
    term_up = factor * contract(up_grad_pre, normed, 0, 0)
    grad_up = sum_at_owner(term_up.astype(jnp.bfloat16), FS, 1)
    grad_rows = jnp.dot(gate_grad_pre, gate_full, preferred_element_type=jnp.float32)
    grad_rows = grad_rows + jnp.dot(up_grad_pre, up_full, preferred_element_type=jnp.float32)
    partial_value = rms_back(grad_rows, unit_rows, inv_rms, gain_rows)
    summed = sum_at_owner(partial_value.astype(jnp.bfloat16), "tp", 1)
    grad_input = (grad_out.astype(jnp.float32) + summed).astype(jnp.bfloat16)
    width_total = gate_weight.shape[1] * lax.axis_size(FS)
    gate_rows, up_rows, down_rows = in_one(
        (
            jnp.sum(grad_gate * grad_gate, axis=1),
            jnp.sum(grad_up * grad_up, axis=1),
            jnp.sum(grad_down * grad_down, axis=1),
        ),
        FS,
    )
    row_squares = jnp.stack([gate_rows, up_rows, down_rows]) / width_total
    return (grad_input, grad_gate, grad_up, grad_down, row_squares)


def solution(mesh):
    split = Mesh(mesh.devices.reshape(8, 4, mesh.shape["tp"]), ("fs_0", "fs_1", "tp"))
    return jax.shard_map(
        on_device,
        mesh=split,
        in_specs=(P(FS, "tp"), P(FS, "tp"), P(), P("tp", FS), P("tp", FS), P("tp", FS)),
        out_specs=(P(FS, "tp"), P("tp", FS), P("tp", FS), P("tp", FS), P(None, "tp")),
        check_vma=False,
    )
```

profile of v0, /device:TPU:8, one launch (start us, length us, event | category | flops | bytes accessed | tf_op | source)
XLA Modules:
  0.0 353.0 jit_solution(1920257956523172577)
XLA Ops:
  7.2 0.0 copy-start.2
  7.2 0.0 all-gather.3.cloned.1.call-start
  7.2 2.3 pad_maximum_fusion
  9.5 0.0 all-gather.3.cloned.1.call-update
  9.5 0.0 all-gather.5.cloned.1.call-start
  9.6 1.5 pad_maximum_fusion.1
  11.1 0.0 all-gather.5.cloned.1.call-update
  11.1 0.0 reduce-scatter.11.cloned.1.call-start
  11.2 57.5 %all-gather.3.cloned.1.call-done = bf16[2048,2048]{1,0:T(8,128)(2,1)} async-done(((bf16[2048,256]{1,0:T(8,128)(2,1)}), bf16[2048,2048]{1,0:T(8,128)(2,1)}) %all-gather.3.cloned.1.call-update) | async-done | bytes 8388624 | tf_op jit(solution)/shard_map/all_gather | solution.py:13
  68.7 3.1 fusion.8
  71.8 84.1 %all-gather.5.cloned.1.call-done = bf16[2048,1152]{1,0:T(8,128)(2,1)} async-done(((bf16[64,1152]{1,0:T(8,128)(2,1)}), bf16[2048,1152]{1,0:T(8,128)(2,1)}) %all-gather.5.cloned.1.call-update) | async-done | bytes 4718608 | tf_op jit(solution)/shard_map/all_gather | solution.py:21
  155.8 0.0 copy-done.2
  155.8 5.2 %fusion.19 = f32[1024,384]{1,0:T(8,128)S(1)} fusion(bf16[2048,1152]{1,0:T(8,128)(2,1)} %all-gather.5.cloned.1.call-done, f32[2048]{0:T(1024)S(1)} %copy-done.2, f32[1024]{0:T(1024)S(1)} %add_rsqrt_fusion, bf16[2048,2048]{1,0:T(8,128)(2,1)} %all-gather.3.cloned.1.call-done), kind=kOutput, calls=%fused_computation.30 | convolution fusion | flops 1619001344 | bytes 7352320 | tf_op jit(solution)/shard_map/dot_general | solution.py:69
  161.1 0.0 slice-start.1
  161.1 5.2 %fusion.22 = f32[1024,384]{1,0:T(8,128)S(1)} fusion(bf16[2048,1152]{1,0:T(8,128)(2,1)} %all-gather.5.cloned.1.call-done, f32[2048]{0:T(1024)S(1)} %copy-done.2, f32[1024]{0:T(1024)S(1)} %add_rsqrt_fusion, bf16[2048,2048]{1,0:T(8,128)(2,1)} %all-gather.3.cloned.1.call-done), kind=kOutput, calls=%fused_computation.33 | convolution fusion | flops 1619001344 | bytes 7352320 | tf_op jit(solution)/shard_map/dot_general | solution.py:69
  166.3 0.0 slice-done
  166.3 0.0 slice-done.1
  166.3 0.0 copy-start.3
  166.3 3.1 multiply_convert_fusion
  169.4 0.0 copy-done.3
  169.4 0.0 reduce-scatter.11.cloned.1.call-update
  169.4 5.9 %multiply_convert_fusion.4 = (bf16[1024,384]{1,0:T(8,128)(2,1)S(1)}, bf16[1024,384]{1,0:T(8,128)(2,1)S(1)}) fusion(f32[1024,384]{1,0:T(8,128)S(1)} %fusion.19, f32[1024,384]{1,0:T(8,128)} %copy-done.3, bf16[2048,1152]{1,0:T(8,128)(2,1)} %all-gather.5.cloned.1.call-done, bf16[2048,2048]{1,0:T(8,128)(2,1)} %all-gather.3.cloned.1.call-done), kind=kOutput, calls=%fused_computation.24 | convolution fusion | flops 1616117760 | bytes 10485760 | tf_op jit(solution)/shard_map/dot_general | solution.py:69
  175.3 4.2 %multiply_convert_fusion.1 = bf16[384,2048]{1,0:T(8,128)(2,1)S(1)} fusion(bf16[1024,384]{1,0:T(8,128)(2,1)S(1)} %get-tuple-element.30, f32[2048]{0:T(1024)S(1)} %copy-done.2, f32[1024]{0:T(1024)S(1)} %add_rsqrt_fusion, bf16[2048,2048]{1,0:T(8,128)(2,1)} %all-gather.3.cloned.1.call-done), kind=kOutput, calls=%fused_computation.20 | convolution fusion | flops 1620574208 | bytes 6565888 | tf_op jit(solution)/shard_map/dot_general | solution.py:69
  179.5 1.6 copy.25
  181.1 5.7 %all-to-all-start.1 = ((bf16[32,384,64]{1,2,0:T(8,128)(2,1)}), bf16[32,384,64]{1,2,0:T(8,128)(2,1)S(1)}, u32[]{:S(2)}, u32[]{:S(2)}) async-start(bf16[32,384,64]{1,2,0:T(8,128)(2,1)} %bitcast.5), calls=%async_computation.2 | async-start | bytes 3145728 | tf_op jit(solution)/shard_map/all_to_all | solution.py:45
  186.8 0.2 reduce-scatter.9.cloned.1.call-start
  187.0 5.4 %multiply_convert_fusion.2 = bf16[384,2048]{1,0:T(8,128)(2,1)} fusion(bf16[1024,384]{1,0:T(8,128)(2,1)S(1)} %get-tuple-element.31, f32[2048]{0:T(1024)S(1)} %copy-done.2, f32[1024]{0:T(1024)S(1)} %add_rsqrt_fusion, bf16[2048,2048]{1,0:T(8,128)(2,1)} %all-gather.3.cloned.1.call-done), kind=kOutput, calls=%fused_computation.21 | convolution fusion | flops 1620574208 | bytes 6565888 | tf_op jit(solution)/shard_map/dot_general | solution.py:69
  192.4 0.0 reduce-scatter.9.cloned.1.call-update
  192.4 0.0 slice-start.2
  192.5 3.9 %fusion.17 = f32[1024,2048]{1,0:T(8,128)S(1)} fusion(bf16[1024,384]{1,0:T(8,128)(2,1)S(1)} %get-tuple-element.31, bf16[2048,1152]{1,0:T(8,128)(2,1)} %all-gather.5.cloned.1.call-done), kind=kOutput, calls=%fused_computation.28 | convolution fusion | flops 1610612736 | bytes 10747904 | tf_op jit(solution)/shard_map/dot_general | solution.py:107
  196.4 0.0 slice-start.3
  196.4 5.7 %fusion.4 = (f32[1024]{0:T(1024)S(1)}, f32[1024,2048]{1,0:T(8,128)S(1)}) fusion(f32[1024]{0:T(1024)S(1)} %add_rsqrt_fusion, bf16[2048,2048]{1,0:T(8,128)(2,1)} %all-gather.3.cloned.1.call-done, f32[1024,2048]{1,0:T(8,128)S(1)} %fusion.17, bf16[1024,384]{1,0:T(8,128)(2,1)S(1)} %get-tuple-element.30, bf16[2048,1152]{1,0:T(8,128)(2,1)} %all-gather.5.cloned.1.call-done, ...), kind=kOutput, calls=%fused_computation.6 | convolution fusion | flops 1623194624 | bytes 23347200 | tf_op jit(solution)/shard_map/dot_general | solution.py:108
  202.1 0.0 slice-done.2
  202.1 0.0 slice-done.3
  202.1 1.8 fusion.7
  203.9 2.2 copy.39
  206.2 25.9 %all-to-all-done.1 = bf16[32,384,64]{1,2,0:T(8,128)(2,1)S(1)} async-done(((bf16[32,384,64]{1,2,0:T(8,128)(2,1)}), bf16[32,384,64]{1,2,0:T(8,128)(2,1)S(1)}, u32[]{:S(2)}, u32[]{:S(2)}) %all-to-all-start.1) | async-done | bytes 1572896 | tf_op jit(solution)/shard_map/all_to_all | solution.py:45
  232.1 5.1 %all-to-all-start = ((bf16[8,1024,256]{2,1,0:T(8,128)(2,1)}), bf16[8,1024,256]{2,1,0:T(8,128)(2,1)}, u32[]{:S(2)}, u32[]{:S(2)}) async-start(bf16[8,1024,256]{2,1,0:T(8,128)(2,1)} %bitcast.25), calls=%async_computation | async-start | bytes 8388608 | tf_op jit(solution)/shard_map/all_to_all | solution.py:45
  237.2 0.0 reduce-scatter.15.cloned.1.call-start
  237.3 1.7 copy.31
  239.0 0.0 reduce-scatter.15.cloned.1.call-update
  239.0 0.0 reduce-scatter.13.cloned.1.call-start
  239.1 34.6 %reduce-scatter.9.cloned.1.call-done = bf16[384,256]{1,0:T(8,128)(2,1)} async-done(((bf16[384,2048]{1,0:T(8,128)(2,1)}), bf16[384,256]{1,0:T(8,128)(2,1)}) %reduce-scatter.9.cloned.1.call-update) | async-done | bytes 196624 | tf_op jit(solution)/shard_map/reduce_scatter | solution.py:34
  273.6 1.7 copy.29
  275.4 0.0 reduce-scatter.13.cloned.1.call-update
  275.4 0.0 copy-start
  275.4 0.2 convert_reduce_fusion.1
  275.6 0.0 copy-start.1
  275.7 22.2 %reduce-scatter.15.cloned.1.call-done = bf16[64,384]{1,0:T(8,128)(2,1)} async-done(((bf16[256,384]{1,0:T(8,128)(2,1)}), bf16[64,384]{1,0:T(8,128)(2,1)}) %reduce-scatter.15.cloned.1.call-update) | async-done | bytes 49168
  297.9 0.9 copy.32
  298.8 0.7 copy.28
  299.6 24.4 %reduce-scatter.13.cloned.1.call-done = bf16[64,384]{1,0:T(8,128)(2,1)} async-done(((bf16[256,384]{1,0:T(8,128)(2,1)}), bf16[64,384]{1,0:T(8,128)(2,1)}) %reduce-scatter.13.cloned.1.call-update) | async-done | bytes 49168
  323.9 0.9 copy.30
  324.8 0.7 copy.27
  325.6 0.2 multiply_reduce_fusion
  325.8 0.0 all-to-all-done
  325.8 0.7 broadcast_in_dim.2
  326.5 8.3 %all-to-all-start.2 = ((f32[32,1,1152]{2,1,0:T(1,128)}), f32[32,1,1152]{2,1,0:T(1,128)S(1)}, u32[]{:S(2)}, u32[]{:S(2)}) async-start(f32[32,1,1152]{2,1,0:T(1,128)} %broadcast_in_dim.2), calls=%async_computation.4 | async-start | bytes 294912 | tf_op jit(solution)/shard_map/all_to_all | solution.py:51
  334.8 2.9 convert_reduce_fusion
  337.7 0.0 copy-done
  337.7 0.9 add_convert_fusion
  338.6 6.7 %all-to-all-done.2 = f32[32,1,1152]{2,1,0:T(1,128)S(1)} async-done(((f32[32,1,1152]{2,1,0:T(1,128)}), f32[32,1,1152]{2,1,0:T(1,128)S(1)}, u32[]{:S(2)}, u32[]{:S(2)}) %all-to-all-start.2) | async-done | bytes 147488 | tf_op jit(solution)/shard_map/all_to_all | solution.py:51
  345.4 0.1 reduce_sum.79
  345.5 0.6 maximum_multiply_fusion
  (13 shorter events, 0.1 us)
Async XLA Ops:
  7.2 148.7 %copy-start.2 = (f32[2048]{0:T(1024)S(1)}, f32[2048]{0:T(1024)}, u32[]{:S(2)}) copy-start(f32[2048]{0:T(1024)} %param.8) | copy-start | bytes 24580
  7.2 61.5 %all-gather.3.cloned.1.call-start = ((), (), s32[]{:S(2)}) async-start(), calls=%async_computation.7 | async-start | bytes 9437184 | tf_op jit(solution)/shard_map/all_gather | solution.py:13
  9.5 146.3 %all-gather.5.cloned.1.call-start = ((), (), s32[]{:S(2)}) async-start(), calls=%async_computation.8 | async-start | bytes 4866048 | tf_op jit(solution)/shard_map/all_gather | solution.py:21
  11.1 226.1 %reduce-scatter.11.cloned.1.call-start = ((), (), s32[]{:S(2)}) async-start(), calls=%async_computation.10 | async-start | bytes 1769472 | tf_op jit(solution)/shard_map/reduce_scatter | solution.py:34
  155.8 10.4 %slice-start = ((s8[8388608]{0:T(1024)(128)(4,1)}), s8[4194304]{0:T(1024)(128)(4,1)S(1)}, s32[]{:S(2)}) async-start(s8[8388608]{0:T(1024)(128)(4,1)} %bitcast.21), calls=%async_computation.13 | async-start | bytes 8388608
  161.1 5.2 %slice-start.1 = ((s8[8388608]{0:T(1024)(128)(4,1)}), s8[4194304]{0:T(1024)(128)(4,1)S(1)}, s32[]{:S(2)}) async-start(s8[8388608]{0:T(1024)(128)(4,1)} %bitcast.21), calls=%async_computation.14 | async-start | bytes 8388608
  166.3 3.1 copy-start.3
  181.1 51.0 %all-to-all-start.1 = ((bf16[32,384,64]{1,2,0:T(8,128)(2,1)}), bf16[32,384,64]{1,2,0:T(8,128)(2,1)S(1)}, u32[]{:S(2)}, u32[]{:S(2)}) async-start(bf16[32,384,64]{1,2,0:T(8,128)(2,1)} %bitcast.5), calls=%async_computation.2 | async-start | bytes 3145728 | tf_op jit(solution)/shard_map/all_to_all | solution.py:45
  186.8 86.8 %reduce-scatter.9.cloned.1.call-start = ((), (), s32[]{:S(2)}) async-start(), calls=%async_computation.9 | async-start | bytes 1769472 | tf_op jit(solution)/shard_map/reduce_scatter | solution.py:34
  192.4 9.6 %slice-start.2 = ((s8[8388608]{0:T(1024)(128)(4,1)}), s8[4194304]{0:T(1024)(128)(4,1)S(1)}, s32[]{:S(2)}) async-start(s8[8388608]{0:T(1024)(128)(4,1)} %bitcast.23), calls=%async_computation.15 | async-start | bytes 8388608
  196.4 5.7 %slice-start.3 = ((s8[8388608]{0:T(1024)(128)(4,1)}), s8[4194304]{0:T(1024)(128)(4,1)S(1)}, s32[]{:S(2)}) async-start(s8[8388608]{0:T(1024)(128)(4,1)} %bitcast.23), calls=%async_computation.16 | async-start | bytes 8388608
  232.1 93.7 %all-to-all-start = ((bf16[8,1024,256]{2,1,0:T(8,128)(2,1)}), bf16[8,1024,256]{2,1,0:T(8,128)(2,1)}, u32[]{:S(2)}, u32[]{:S(2)}) async-start(bf16[8,1024,256]{2,1,0:T(8,128)(2,1)} %bitcast.25), calls=%async_computation | async-start | bytes 8388608 | tf_op jit(solution)/shard_map/all_to_all | solution.py:45
  237.2 60.7 %reduce-scatter.15.cloned.1.call-start = ((), (), s32[]{:S(2)}) async-start(), calls=%async_computation.12 | async-start | bytes 245760
  239.0 84.9 %reduce-scatter.13.cloned.1.call-start = ((), (), s32[]{:S(2)}) async-start(), calls=%async_computation.11 | async-start | bytes 245760
  275.4 62.3 %copy-start = (bf16[1024,256]{1,0:T(8,128)(2,1)S(1)}, bf16[1024,256]{1,0:T(8,128)(2,1)}, u32[]{:S(2)}) copy-start(bf16[1024,256]{1,0:T(8,128)(2,1)} %param.7) | copy-start | bytes 1572868
  275.6 63.0 %copy-start.1 = (f32[384,64]{0,1:T(8,128)}, f32[384,64]{0,1:T(8,128)S(1)}, u32[]{:S(2)}) copy-start(f32[384,64]{0,1:T(8,128)S(1)} %convert_reduce_fusion.1) | copy-start | bytes 294916
  326.5 18.9 %all-to-all-start.2 = ((f32[32,1,1152]{2,1,0:T(1,128)}), f32[32,1,1152]{2,1,0:T(1,128)S(1)}, u32[]{:S(2)}, u32[]{:S(2)}) async-start(f32[32,1,1152]{2,1,0:T(1,128)} %broadcast_in_dim.2), calls=%async_computation.4 | async-start | bytes 294912 | tf_op jit(solution)/shard_map/all_to_all | solution.py:51
Sparse Core Ops, SparseCore 0:
  9.8 58.8 all-gather.2
  71.8 83.9 all-gather.4
  169.5 56.4 reduce-scatter.10
  228.4 45.1 reduce-scatter.8
  276.0 21.8 reduce-scatter.14
  300.8 23.0 reduce-scatter.12
where the time goes:
time: 354 us; the launch traced here: 353 us
  waiting for transfers between devices  256 us (72%)
  matrix products  38.6 us (11%)
  starting transfers between devices  19.5 us (6%)
  between operations  14.4 us (4%)
  other arithmetic  13.6 us (4%)
  local copies, waits for them, and re-layouts  11.4 us (3%)
    all_gather x1, waiting for transfers between devices, gather_turned(): whole = lax.all_gather(both, axis, axis=0, tiled=True)  84.1 us
    all_gather x1, waiting for transfers between devices, sent_together(): whole = lax.all_gather(both, axis, axis=dim, tiled=True)  57.5 us
    unnamed x8, waiting for transfers between devices  46.7 us
    reduce_scatter x2, waiting for transfers between devices, summed_rows(): nearer = lax.psum_scatter(x, axes[0], scatter_dimension=dim, tiled=True)  34.6 us
    dot_general x6, matrix products, contract(): lax.dot_general(left, right, (((left_dim,), (right_dim,)), ((), ())), pre...  29 us
    all_to_all x2, waiting for transfers between devices, sum_at_owner(): parts = lax.all_to_all(in_blocks(x, dim, peers), axis, 0, 0, tiled=True)  25.9 us
    all_to_all x2, starting transfers between devices, sum_at_owner(): parts = lax.all_to_all(in_blocks(x, dim, peers), axis, 0, 0, tiled=True)  10.8 us
    all_to_all x1, starting transfers between devices, copy_for_each(): lax.all_to_all(jnp.broadcast_to(x[None], (peers, *x.shape)), axis, 0, 0,...  8.32 us
  transfers between devices with their start and end apart: 9, of which 7 were waited for; matrix products, arithmetic and copies ran while one was open for 13% of the time, Pallas kernels for 0%

commit v1 on v0

--- a/solution.py
+++ b/solution.py
@@ -5,6 +5,11 @@
 from jax.sharding import PartitionSpec as P
 
 FS = ("fs_0", "fs_1")
+
+
+def all_by_exchange(x, axis, dim):
+    sent = jnp.stack([x] * lax.axis_size(axis))
+    return jnp.concatenate(lax.all_to_all(sent, axis, 0, 0), axis=dim)
 
 
 def sent_together(arrays, axis, dim, along):
@@ -18,7 +23,7 @@
     turned = [jnp.moveaxis(a, dim, 0) for a, dim in zip(arrays, dims)]
     widths = [t[0].size for t in turned]
     both = jnp.concatenate([t.reshape(-1, w) for t, w in zip(turned, widths)], axis=1)
-    whole = lax.all_gather(both, axis, axis=0, tiled=True)
+    whole = all_by_exchange(both, axis, 0)
     parts = jnp.split(whole, [sum(widths[:k]) for k in range(1, len(widths))], axis=1)
     return tuple(
         (

time: 354 us -> 324 us (0.915)
  waiting for transfers between devices: 256 us -> 211 us
  starting transfers between devices: 19.5 us -> 33.7 us
    all_gather x1 -> x0, waiting for transfers between devices: 84.1 us -> none  [gather_turned(): whole = lax.all_gather(both, axis, axis=0, tiled=True)]
    all_to_all x0 -> x1, waiting for transfers between devices: none -> 58 us  [all_by_exchange(): return jnp.concatenate(lax.all_to_all(sent, axis, 0, 0), axis=dim)]
    all_gather x1, waiting for transfers between devices: 57.5 us -> 44 us  [sent_together(): whole = lax.all_gather(both, axis, axis=dim, tiled=True)]
    all_to_all x0 -> x1, starting transfers between devices: none -> 11.4 us  [all_by_exchange(): return jnp.concatenate(lax.all_to_all(sent, axis, 0, 0), axis=dim)]
    reduce_scatter x2, waiting for transfers between devices: 34.6 us -> 27.3 us  [summed_rows(): nearer = lax.psum_scatter(x, axes[0], scatter_dimension=dim, tiled=True)]
    unnamed x8 -> x7, waiting for transfers between devices: 46.7 us -> 46.6 us
  transfers between devices with their start and end apart: 9 -> 9, of which waited for: 7 -> 7; matrix products, arithmetic and copies ran while one was open for 13% -> 15% of each run, Pallas kernels for 0% -> 0%
where the time goes in v1:
time: 324 us; the launch traced here: 323 us
  waiting for transfers between devices  211 us (65%)
  matrix products  37.1 us (11%)
  starting transfers between devices  33.7 us (10%)
  local copies, waits for them, and re-layouts  14.1 us (4%)
  between operations  14 us (4%)
  other arithmetic  13 us (4%)
    all_to_all x1, waiting for transfers between devices, all_by_exchange(): return jnp.concatenate(lax.all_to_all(sent, axis, 0, 0), axis=dim)  58 us
    unnamed x7, waiting for transfers between devices  46.6 us
    all_gather x1, waiting for transfers between devices, sent_together(): whole = lax.all_gather(both, axis, axis=dim, tiled=True)  44 us
    all_to_all x2, waiting for transfers between devices, sum_at_owner(): parts = lax.all_to_all(in_blocks(x, dim, peers), axis, 0, 0, tiled=True)  28.3 us
    dot_general x6, matrix products, contract(): lax.dot_general(left, right, (((left_dim,), (right_dim,)), ((), ())), pre...  27.6 us
    reduce_scatter x2, waiting for transfers between devices, summed_rows(): nearer = lax.psum_scatter(x, axes[0], scatter_dimension=dim, tiled=True)  27.3 us
    all_to_all x2, starting transfers between devices, sum_at_owner(): parts = lax.all_to_all(in_blocks(x, dim, peers), axis, 0, 0, tiled=True)  13.8 us
    all_to_all x1, starting transfers between devices, all_by_exchange(): return jnp.concatenate(lax.all_to_all(sent, axis, 0, 0), axis=dim)  11.4 us
  transfers between devices with their start and end apart: 9, of which 7 were waited for; matrix products, arithmetic and copies ran while one was open for 15% of the time, Pallas kernels for 0%

profile of v1, /device:TPU:8, one launch (start us, length us, event | category | flops | bytes accessed | tf_op | source)
XLA Modules:
  0.0 323.0 jit_solution(10811816415289694159)
XLA Ops:
  7.2 0.0 all-gather.2.cloned.1.call-start
  7.2 2.3 pad_maximum_fusion
  9.5 0.0 all-gather.2.cloned.1.call-update
  9.5 0.9 pad_maximum_fusion.1
  10.4 2.7 stack.10
  13.1 11.4 %all-to-all-start = ((bf16[32,64,1152]{2,1,0:T(8,128)(2,1)}), bf16[32,64,1152]{2,1,0:T(8,128)(2,1)}, u32[]{:S(2)}, u32[]{:S(2)}) async-start(bf16[32,64,1152]{2,1,0:T(8,128)(2,1)} %stack.10), calls=%async_computation | async-start | bytes 9437184 | tf_op jit(solution)/shard_map/all_to_all | solution.py:12
  24.6 0.0 copy-start.3
  24.6 0.0 reduce-scatter.11.cloned.1.call-start
  24.6 44.0 %all-gather.2.cloned.1.call-done = bf16[2048,2048]{1,0:T(8,128)(2,1)} async-done(((bf16[2048,256]{1,0:T(8,128)(2,1)}), bf16[2048,2048]{1,0:T(8,128)(2,1)}) %all-gather.2.cloned.1.call-update) | async-done | bytes 8388624 | tf_op jit(solution)/shard_map/all_gather | solution.py:18
  68.7 3.1 fusion.8
  71.8 58.0 %all-to-all-done = bf16[32,64,1152]{2,1,0:T(8,128)(2,1)} async-done(((bf16[32,64,1152]{2,1,0:T(8,128)(2,1)}), bf16[32,64,1152]{2,1,0:T(8,128)(2,1)}, u32[]{:S(2)}, u32[]{:S(2)}) %all-to-all-start) | async-done | bytes 4718624 | tf_op jit(solution)/shard_map/all_to_all | solution.py:12
  129.8 0.0 copy-done.3
  129.8 5.2 %fusion.19 = f32[1024,384]{1,0:T(8,128)S(1)} fusion(bf16[2048,1152]{1,0:T(8,128)(2,1)} %bitcast.3, f32[2048]{0:T(1024)S(1)} %copy-done.3, f32[1024]{0:T(1024)S(1)} %add_rsqrt_fusion, bf16[2048,2048]{1,0:T(8,128)(2,1)} %all-gather.2.cloned.1.call-done), kind=kOutput, calls=%fused_computation.30 | convolution fusion | flops 1619001344 | bytes 7352320 | tf_op jit(solution)/shard_map/dot_general | solution.py:74
  135.0 0.0 copy-done
  135.0 3.8 %fusion.22 = f32[1024,384]{1,0:T(8,128)S(1)} fusion(bf16[2048,1152]{1,0:T(8,128)(2,1)} %bitcast.3, f32[2048]{0:T(1024)S(1)} %copy-done.3, f32[1024]{0:T(1024)S(1)} %add_rsqrt_fusion, bf16[2048,2048]{1,0:T(8,128)(2,1)S(1)} %copy-done), kind=kOutput, calls=%fused_computation.33 | convolution fusion | flops 1619001344 | bytes 7352320 | tf_op jit(solution)/shard_map/dot_general | solution.py:74
  138.8 0.0 copy-start.4
  138.8 3.1 multiply_convert_fusion
  141.9 0.0 copy-done.4
  141.9 0.0 reduce-scatter.11.cloned.1.call-update
  141.9 5.9 %multiply_convert_fusion.4 = (bf16[1024,384]{1,0:T(8,128)(2,1)S(1)}, bf16[1024,384]{1,0:T(8,128)(2,1)S(1)}) fusion(f32[1024,384]{1,0:T(8,128)S(1)} %fusion.19, f32[1024,384]{1,0:T(8,128)} %copy-done.4, bf16[2048,1152]{1,0:T(8,128)(2,1)} %bitcast.3, bf16[2048,2048]{1,0:T(8,128)(2,1)} %all-gather.2.cloned.1.call-done), kind=kOutput, calls=%fused_computation.24 | convolution fusion | flops 1616117760 | bytes 10485760 | tf_op jit(solution)/shard_map/dot_general | solution.py:74
  147.8 4.2 %multiply_convert_fusion.1 = bf16[384,2048]{1,0:T(8,128)(2,1)S(1)} fusion(bf16[1024,384]{1,0:T(8,128)(2,1)S(1)} %get-tuple-element.30, f32[2048]{0:T(1024)S(1)} %copy-done.3, f32[1024]{0:T(1024)S(1)} %add_rsqrt_fusion, bf16[2048,2048]{1,0:T(8,128)(2,1)} %all-gather.2.cloned.1.call-done), kind=kOutput, calls=%fused_computation.20 | convolution fusion | flops 1620574208 | bytes 6565888 | tf_op jit(solution)/shard_map/dot_general | solution.py:74
  152.0 1.6 copy.25
  153.6 8.8 %all-to-all-start.2 = ((bf16[32,384,64]{1,2,0:T(8,128)(2,1)}), bf16[32,384,64]{1,2,0:T(8,128)(2,1)S(1)}, u32[]{:S(2)}, u32[]{:S(2)}) async-start(bf16[32,384,64]{1,2,0:T(8,128)(2,1)} %bitcast.6), calls=%async_computation.3 | async-start | bytes 3145728 | tf_op jit(solution)/shard_map/all_to_all | solution.py:50
  162.5 0.0 reduce-scatter.9.cloned.1.call-start
  162.5 5.4 %multiply_convert_fusion.2 = bf16[384,2048]{1,0:T(8,128)(2,1)} fusion(bf16[1024,384]{1,0:T(8,128)(2,1)S(1)} %get-tuple-element.31, f32[2048]{0:T(1024)S(1)} %copy-done.3, f32[1024]{0:T(1024)S(1)} %add_rsqrt_fusion, bf16[2048,2048]{1,0:T(8,128)(2,1)} %all-gather.2.cloned.1.call-done), kind=kOutput, calls=%fused_computation.21 | convolution fusion | flops 1620574208 | bytes 6565888 | tf_op jit(solution)/shard_map/dot_general | solution.py:74
  167.9 0.0 reduce-scatter.9.cloned.1.call-update
  167.9 0.0 slice-start
  167.9 3.9 %fusion.17 = f32[1024,2048]{1,0:T(8,128)S(1)} fusion(bf16[1024,384]{1,0:T(8,128)(2,1)S(1)} %get-tuple-element.31, bf16[2048,1152]{1,0:T(8,128)(2,1)} %bitcast.3), kind=kOutput, calls=%fused_computation.28 | convolution fusion | flops 1610612736 | bytes 10747904 | tf_op jit(solution)/shard_map/dot_general | solution.py:112
  171.9 0.0 slice-start.1
  171.9 5.6 %fusion.4 = (f32[1024]{0:T(1024)S(1)}, f32[1024,2048]{1,0:T(8,128)S(1)}) fusion(f32[1024]{0:T(1024)S(1)} %add_rsqrt_fusion, bf16[2048,2048]{1,0:T(8,128)(2,1)} %all-gather.2.cloned.1.call-done, f32[1024,2048]{1,0:T(8,128)S(1)} %fusion.17, bf16[1024,384]{1,0:T(8,128)(2,1)S(1)} %get-tuple-element.30, bf16[2048,1152]{1,0:T(8,128)(2,1)} %bitcast.3, ...), kind=kOutput, calls=%fused_computation.6 | convolution fusion | flops 1623194624 | bytes 23347200 | tf_op jit(solution)/shard_map/dot_general | solution.py:113
  177.5 0.0 slice-done
  177.6 0.0 slice-done.1
  177.6 1.8 fusion.7
  179.4 2.2 copy.39
  181.6 28.3 %all-to-all-done.2 = bf16[32,384,64]{1,2,0:T(8,128)(2,1)S(1)} async-done(((bf16[32,384,64]{1,2,0:T(8,128)(2,1)}), bf16[32,384,64]{1,2,0:T(8,128)(2,1)S(1)}, u32[]{:S(2)}, u32[]{:S(2)}) %all-to-all-start.2) | async-done | bytes 1572896 | tf_op jit(solution)/shard_map/all_to_all | solution.py:50
  210.0 5.0 %all-to-all-start.1 = ((bf16[8,1024,256]{2,1,0:T(8,128)(2,1)}), bf16[8,1024,256]{2,1,0:T(8,128)(2,1)}, u32[]{:S(2)}, u32[]{:S(2)}) async-start(bf16[8,1024,256]{2,1,0:T(8,128)(2,1)} %bitcast.24), calls=%async_computation.1 | async-start | bytes 8388608 | tf_op jit(solution)/shard_map/all_to_all | solution.py:50
  214.9 0.0 reduce-scatter.15.cloned.1.call-start
  214.9 0.0 reduce-scatter.11.cloned.1.call-done
  214.9 1.8 copy.31
  216.7 0.0 reduce-scatter.15.cloned.1.call-update
  216.7 0.0 reduce-scatter.13.cloned.1.call-start
  216.8 27.3 %reduce-scatter.9.cloned.1.call-done = bf16[384,256]{1,0:T(8,128)(2,1)} async-done(((bf16[384,2048]{1,0:T(8,128)(2,1)}), bf16[384,256]{1,0:T(8,128)(2,1)}) %reduce-scatter.9.cloned.1.call-update) | async-done | bytes 196624 | tf_op jit(solution)/shard_map/reduce_scatter | solution.py:39
  244.1 1.7 copy.29
  245.8 0.0 reduce-scatter.13.cloned.1.call-update
  245.8 0.0 copy-start.1
  245.9 0.2 convert_reduce_fusion.1
  246.1 0.0 copy-start.2
  246.1 22.2 %reduce-scatter.15.cloned.1.call-done = bf16[64,384]{1,0:T(8,128)(2,1)} async-done(((bf16[256,384]{1,0:T(8,128)(2,1)}), bf16[64,384]{1,0:T(8,128)(2,1)}) %reduce-scatter.15.cloned.1.call-update) | async-done | bytes 49168
  268.3 0.9 copy.32
  269.3 0.7 copy.28
  270.0 24.3 %reduce-scatter.13.cloned.1.call-done = bf16[64,384]{1,0:T(8,128)(2,1)} async-done(((bf16[256,384]{1,0:T(8,128)(2,1)}), bf16[64,384]{1,0:T(8,128)(2,1)}) %reduce-scatter.13.cloned.1.call-update) | async-done | bytes 49168
  294.3 0.9 copy.30
  295.2 0.7 copy.27
  295.9 0.2 multiply_reduce_fusion
  296.1 0.0 all-to-all-done.1
  296.1 0.7 broadcast_in_dim.2
  296.9 8.3 %all-to-all-start.3 = ((f32[32,1,1152]{2,1,0:T(1,128)}), f32[32,1,1152]{2,1,0:T(1,128)S(1)}, u32[]{:S(2)}, u32[]{:S(2)}) async-start(f32[32,1,1152]{2,1,0:T(1,128)} %broadcast_in_dim.2), calls=%async_computation.5 | async-start | bytes 294912 | tf_op jit(solution)/shard_map/all_to_all | solution.py:56
  305.2 2.9 convert_reduce_fusion
  308.0 0.0 copy-done.1
  308.0 0.9 add_convert_fusion
  308.9 0.0 copy-done.2
  309.0 6.8 %all-to-all-done.3 = f32[32,1,1152]{2,1,0:T(1,128)S(1)} async-done(((f32[32,1,1152]{2,1,0:T(1,128)}), f32[32,1,1152]{2,1,0:T(1,128)S(1)}, u32[]{:S(2)}, u32[]{:S(2)}) %all-to-all-start.3) | async-done | bytes 147488 | tf_op jit(solution)/shard_map/all_to_all | solution.py:56
  315.7 0.1 reduce_sum.79
  315.9 0.6 maximum_multiply_fusion
  (10 shorter events, 0.1 us)
Async XLA Ops:
  7.2 61.5 %all-gather.2.cloned.1.call-start = ((), (), s32[]{:S(2)}) async-start(), calls=%async_computation.8 | async-start | bytes 9437184 | tf_op jit(solution)/shard_map/all_gather | solution.py:18
  13.1 116.6 %all-to-all-start = ((bf16[32,64,1152]{2,1,0:T(8,128)(2,1)}), bf16[32,64,1152]{2,1,0:T(8,128)(2,1)}, u32[]{:S(2)}, u32[]{:S(2)}) async-start(bf16[32,64,1152]{2,1,0:T(8,128)(2,1)} %stack.10), calls=%async_computation | async-start | bytes 9437184 | tf_op jit(solution)/shard_map/all_to_all | solution.py:12
  24.6 105.2 %copy-start.3 = (f32[2048]{0:T(1024)S(1)}, f32[2048]{0:T(1024)}, u32[]{:S(2)}) copy-start(f32[2048]{0:T(1024)} %param.8) | copy-start | bytes 24580
  24.6 190.3 %reduce-scatter.11.cloned.1.call-start = ((), (), s32[]{:S(2)}) async-start(), calls=%async_computation.10 | async-start | bytes 1769472 | tf_op jit(solution)/shard_map/reduce_scatter | solution.py:39
  129.8 5.2 %copy-start = (bf16[2048,2048]{1,0:T(8,128)(2,1)S(1)}, bf16[2048,2048]{1,0:T(8,128)(2,1)}, u32[]{:S(2)}) copy-start(bf16[2048,2048]{1,0:T(8,128)(2,1)} %all-gather.2.cloned.1.call-done) | copy-start | bytes 25165828
  138.8 3.1 copy-start.4
  153.6 56.4 %all-to-all-start.2 = ((bf16[32,384,64]{1,2,0:T(8,128)(2,1)}), bf16[32,384,64]{1,2,0:T(8,128)(2,1)S(1)}, u32[]{:S(2)}, u32[]{:S(2)}) async-start(bf16[32,384,64]{1,2,0:T(8,128)(2,1)} %bitcast.6), calls=%async_computation.3 | async-start | bytes 3145728 | tf_op jit(solution)/shard_map/all_to_all | solution.py:50
  162.5 81.6 %reduce-scatter.9.cloned.1.call-start = ((), (), s32[]{:S(2)}) async-start(), calls=%async_computation.9 | async-start | bytes 1769472 | tf_op jit(solution)/shard_map/reduce_scatter | solution.py:39
  167.9 9.6 %slice-start = ((s8[8388608]{0:T(1024)(128)(4,1)}), s8[4194304]{0:T(1024)(128)(4,1)S(1)}, s32[]{:S(2)}) async-start(s8[8388608]{0:T(1024)(128)(4,1)} %bitcast.22), calls=%async_computation.13 | async-start | bytes 8388608
  171.9 5.7 %slice-start.1 = ((s8[8388608]{0:T(1024)(128)(4,1)}), s8[4194304]{0:T(1024)(128)(4,1)S(1)}, s32[]{:S(2)}) async-start(s8[8388608]{0:T(1024)(128)(4,1)} %bitcast.22), calls=%async_computation.14 | async-start | bytes 8388608
  210.0 86.2 %all-to-all-start.1 = ((bf16[8,1024,256]{2,1,0:T(8,128)(2,1)}), bf16[8,1024,256]{2,1,0:T(8,128)(2,1)}, u32[]{:S(2)}, u32[]{:S(2)}) async-start(bf16[8,1024,256]{2,1,0:T(8,128)(2,1)} %bitcast.24), calls=%async_computation.1 | async-start | bytes 8388608 | tf_op jit(solution)/shard_map/all_to_all | solution.py:50
  214.9 53.4 %reduce-scatter.15.cloned.1.call-start = ((), (), s32[]{:S(2)}) async-start(), calls=%async_computation.12 | async-start | bytes 245760
  216.7 77.6 %reduce-scatter.13.cloned.1.call-start = ((), (), s32[]{:S(2)}) async-start(), calls=%async_computation.11 | async-start | bytes 245760
  245.8 62.2 %copy-start.1 = (bf16[1024,256]{1,0:T(8,128)(2,1)S(1)}, bf16[1024,256]{1,0:T(8,128)(2,1)}, u32[]{:S(2)}) copy-start(bf16[1024,256]{1,0:T(8,128)(2,1)} %param.7) | copy-start | bytes 1572868
  246.1 62.9 %copy-start.2 = (f32[384,64]{0,1:T(8,128)}, f32[384,64]{0,1:T(8,128)S(1)}, u32[]{:S(2)}) copy-start(f32[384,64]{0,1:T(8,128)S(1)} %convert_reduce_fusion.1) | copy-start | bytes 294916
  296.9 18.8 %all-to-all-start.3 = ((f32[32,1,1152]{2,1,0:T(1,128)}), f32[32,1,1152]{2,1,0:T(1,128)S(1)}, u32[]{:S(2)}, u32[]{:S(2)}) async-start(f32[32,1,1152]{2,1,0:T(1,128)} %broadcast_in_dim.2), calls=%async_computation.5 | async-start | bytes 294912 | tf_op jit(solution)/shard_map/all_to_all | solution.py:56
Sparse Core Ops, SparseCore 0:
  9.8 58.8 all-gather.1
  142.0 57.7 reduce-scatter.10
  202.4 41.6 reduce-scatter.8
  246.4 21.8 reduce-scatter.14
  271.3 22.9 reduce-scatter.12
